TPU v7x, 32 devices: a whole 2x2x4 slice. The times are simulated.
32 devices in a mesh: pp: 2 (over x), fs: 4 (over y, core), tp: 4 (over z).
Axes of the slice: x: 2, y: 2, z: 4, core: 2. Of those that a mesh axis runs over, the one named last changes fastest.
Arguments:
- inputs: bfloat16 [512, 2048], P('pp', ('fs', 'tp')), may hold values from -6 to 6
- norm_gain: bfloat16 [2, 2048], P('pp', ('fs', 'tp')), may hold values from 0.099609375 to 1.8984375
- w_value: bfloat16 [2, 2048, 2048], P('pp', None, ('fs', 'tp')), may hold values from -0.125 to 0.125
- w_gate: bfloat16 [2, 2048, 2048], P('pp', None, ('fs', 'tp')), may hold values from -0.125 to 0.125
- w_taps: bfloat16 [2, 31, 2048], P('pp', None, ('fs', 'tp')), may hold values from -1 to 1
- ln_gain: float32 [2, 2048], P('pp', ('fs', 'tp')), may hold values from 0.1 to 1.9
- ln_shift: float32 [2, 2048], P('pp', ('fs', 'tp')), may hold values from -3 to 3
Outputs:
- outputs: bfloat16 [512, 2048], P('pp', ('fs', 'tp'))
All inputs are finite; a program needn't handle non-finite values.
Results may differ from a plain program's by a relative error of at most 0.0085.
Values may be sent and summed in bfloat16 or wider, within the bound.
A program may use at most 64 MiB of HBM per device.

v0:
```python
import jax
import jax.numpy as jnp
from jax import lax
from jax.sharding import PartitionSpec as P

LEN = 128
norm_eps = 1e-06
layer_eps = 1e-05


def from_behind(block, axis, distance):
    devices = range(lax.axis_size(axis))
    route = [(i - distance, i) for i in devices if i - distance in devices]
    return lax.ppermute(block, axis, route)


def local(inputs, norm_gain, w_value, w_gate, w_taps, ln_gain, ln_shift):
    num_sections = lax.axis_size("pp")
    my_section = lax.axis_index("pp")
    model_width = w_value.shape[1]
    channels = w_value.shape[2]
    tap_count = w_taps.shape[1]
    fed_rows = lax.all_gather(inputs, "pp", axis=0, tiled=True)
    total_rows = fed_rows.shape[0]
    block_rows = LEN
    per_batch = LEN // block_rows
    block_count = total_rows // block_rows
    step_count = block_count + num_sections - 1
    gain_row = norm_gain[0]
    value_weight = w_value[0]
    gate_weight = w_gate[0]
    tap_weights = w_taps[0].astype(jnp.float32)
    layer_gain = ln_gain[0]
    layer_shift = ln_shift[0]

    def convolve(operands):
        history, gated_rows = operands
        padded = jnp.concatenate([history, gated_rows], axis=0)
        convolved = jnp.zeros((block_rows, channels), jnp.float32)
        for tap_index in range(tap_count):
            convolved = (
                convolved + padded[tap_index : tap_index + block_rows] * tap_weights[tap_index]
            )
        return convolved

    def skip_convolve(operands):
        return jnp.zeros((block_rows, channels), jnp.float32)

    def process_block(stream, history, active):
        stream_f = stream.astype(jnp.float32)
        zero_block = jnp.zeros((block_rows, channels), jnp.float32)
        squares = lax.psum(jnp.sum(stream_f * stream_f, axis=1), ("fs", "tp"))
        scale_rows = lax.rsqrt(squares / model_width + norm_eps)[:, None]
        normed = (stream_f * scale_rows * gain_row.astype(jnp.float32)).astype(jnp.bfloat16)
        shard_piece = lax.all_gather(normed, ("fs", "tp"), axis=1, tiled=True)

        def accumulate(current):
            return (
                jnp.dot(shard_piece, value_weight, preferred_element_type=jnp.float32),
                jnp.dot(shard_piece, gate_weight, preferred_element_type=jnp.float32),
            )

        def unchanged(current):
            return current

        value_sum, gate_sum = lax.cond(active, accumulate, unchanged, (zero_block, zero_block))
        gated_rows = value_sum * jax.nn.sigmoid(gate_sum)
        convolved = lax.cond(active, convolve, skip_convolve, (history, gated_rows))
        new_history = jnp.where(
            active, jnp.concatenate([history, gated_rows], axis=0)[block_rows:], history
        )
        moments = lax.psum(
            (jnp.sum(convolved, axis=1), jnp.sum(convolved * convolved, axis=1)), ("fs", "tp")
        )
        row_mean = moments[0][:, None] / model_width
        row_var = moments[1][:, None] / model_width - row_mean * row_mean
        normed_conv = (convolved - row_mean) * lax.rsqrt(
            row_var + layer_eps
        ) * layer_gain + layer_shift
        new_stream = (stream_f + jax.nn.silu(normed_conv)).astype(jnp.bfloat16)
        return (jnp.where(active, new_stream, stream), new_history)

    def step_body(step_index, loop_state):
        stream, history, results = loop_state
        block_index = step_index - my_section
        active = (block_index >= 0) & (block_index < block_count)
        safe_index = jnp.clip(block_index, 0, block_count - 1)
        row_offset = safe_index * block_rows
        first_rows = lax.dynamic_slice_in_dim(fed_rows, row_offset, block_rows, 0)
        stream = jnp.where(my_section == 0, first_rows, stream)
        history = jnp.where(
            active & (safe_index % per_batch == 0), jnp.zeros_like(history), history
        )
        new_stream, new_history = process_block(stream, history, active)
        previous = lax.dynamic_slice_in_dim(results, row_offset, block_rows, 0)
        keep_rows = active & (my_section == num_sections - 1)
        results = lax.dynamic_update_slice_in_dim(
            results, jnp.where(keep_rows, new_stream, previous), row_offset, 0
        )
        passed = from_behind(new_stream, "pp", 1)
        return (passed, new_history, results)

    initial = (
        jnp.zeros((block_rows, channels), jnp.bfloat16),
        jnp.zeros((tap_count - 1, channels), jnp.float32),
        jnp.zeros((total_rows, channels), jnp.bfloat16),
    )
    final_state = lax.fori_loop(0, step_count, step_body, initial)
    own_rows = inputs.shape[0]
    shares = final_state[2].reshape(num_sections, own_rows, channels)
    arrived = lax.all_to_all(shares, "pp", split_axis=0, concat_axis=0, tiled=True)
    return arrived[num_sections - 1]


def solution(mesh):
    in_specs = (
        P("pp", ("fs", "tp")),
        P("pp", ("fs", "tp")),
        P("pp", None, ("fs", "tp")),
        P("pp", None, ("fs", "tp")),
        P("pp", None, ("fs", "tp")),
        P("pp", ("fs", "tp")),
        P("pp", ("fs", "tp")),
    )
    out_specs = P("pp", ("fs", "tp"))
    return jax.shard_map(local, mesh=mesh, in_specs=in_specs, out_specs=out_specs, check_vma=False)
```

profile of v0, /device:TPU:0, one launch (start us, length us, event | category | flops | bytes accessed | tf_op | source)
XLA Modules:
  0.0 539.6 jit_solution(15302463253678728073)
XLA Ops:
  0.0 6.3 %all_gather.13 = bf16[512,128]{1,0:T(8,128)(2,1)S(1)} all-gather(bf16[256,128]{1,0:T(8,128)(2,1)} %param.13), channel_id=1, replica_groups=mesh['pp'=2,'fs'=4,'tp'=4] {'pp'}, dimensions={0}, use_global_device_ids=true | all-gather | bytes 196608 | tf_op jit(solution)/shard_map/all_gather | solution.py:23
  7.0 524.0 %while.20 = (s32[]{:T(128)}, bf16[128,128]{1,0:T(8,128)(2,1)S(1)}, f32[30,128]{1,0:T(8,128)S(1)}, bf16[512,128]{1,0:T(8,128)(2,1)S(1)}, s32[]{:T(128)}, /*index=...) while((s32[]{:T(128)}, bf16[128,128]{1,0:T(8,128)(2,1)S(1)}, ...), condition=%wide.region_11.12_spmd.clone, body=%wide.region_0.11_spmd.clone.sunk | while | flops 136179984 | bytes 5903558 | solution.py:108
  7.1 33.1 %psum.46 = f32[128]{0:T(128)S(1)} all-reduce(f32[128]{0:T(128)S(1)} %get-tuple-element.554), channel_id=1, replica_groups=mesh['pp'=2,'fs'=4,'tp'=4] {'fs','tp'}, use_global_device_ids=true, to_apply=%region_2.2 | all-reduce | flops 128 | bytes 1024 | tf_op jit(solution)/shard_map/while/body/eval_jaxpr/psum | solution.py:52
  40.3 33.2 %all_gather.16 = bf16[128,2048]{1,0:T(8,128)(2,1)S(1)} all-gather(bf16[128,128]{1,0:T(8,128)(2,1)S(1)} %fusion.106), channel_id=1, replica_groups=mesh['pp'=2,'fs'=4,'tp'=4] {'fs','tp'}, dimensions={1}, use_global_device_ids=true | all-gather | bytes 557056 | tf_op jit(solution)/shard_map/while/body/eval_jaxpr/all_gather | solution.py:55
  73.5 1.6 conditional.6
  75.6 31.4 %all-reduce.2 = (f32[128]{0:T(128)S(1)}, f32[128]{0:T(128)S(1)}) all-reduce(f32[128]{0:T(128)S(1)} %get-tuple-element.558, f32[128]{0:T(128)S(1)} %get-tuple-element.559), channel_id=1, replica_groups=mesh['pp'=2,'fs'=4,'tp'=4] {'fs','tp'}, use_global_device_ids=true, to_apply=%region_10.10 | all-reduce | flops 256 | bytes 2048 | tf_op jit(solution)/shard_map/while/body/eval_jaxpr/psum | solution.py:72
  107.1 1.7 collective-permute-start
  108.8 1.6 collective-permute-done
  110.5 30.2 %psum.46 = f32[128]{0:T(128)S(1)} all-reduce(f32[128]{0:T(128)S(1)} %get-tuple-element.554), channel_id=1, replica_groups=mesh['pp'=2,'fs'=4,'tp'=4] {'fs','tp'}, use_global_device_ids=true, to_apply=%region_2.2 | all-reduce | flops 128 | bytes 1024 | tf_op jit(solution)/shard_map/while/body/eval_jaxpr/psum | solution.py:52
  140.8 36.4 %all_gather.16 = bf16[128,2048]{1,0:T(8,128)(2,1)S(1)} all-gather(bf16[128,128]{1,0:T(8,128)(2,1)S(1)} %fusion.106), channel_id=1, replica_groups=mesh['pp'=2,'fs'=4,'tp'=4] {'fs','tp'}, dimensions={1}, use_global_device_ids=true | all-gather | bytes 557056 | tf_op jit(solution)/shard_map/while/body/eval_jaxpr/all_gather | solution.py:55
  177.2 1.6 conditional.6
  179.2 29.7 %all-reduce.2 = (f32[128]{0:T(128)S(1)}, f32[128]{0:T(128)S(1)}) all-reduce(f32[128]{0:T(128)S(1)} %get-tuple-element.558, f32[128]{0:T(128)S(1)} %get-tuple-element.559), channel_id=1, replica_groups=mesh['pp'=2,'fs'=4,'tp'=4] {'fs','tp'}, use_global_device_ids=true, to_apply=%region_10.10 | all-reduce | flops 256 | bytes 2048 | tf_op jit(solution)/shard_map/while/body/eval_jaxpr/psum | solution.py:72
  209.1 4.2 collective-permute-start
  213.3 1.6 collective-permute-done
  215.0 32.0 %psum.46 = f32[128]{0:T(128)S(1)} all-reduce(f32[128]{0:T(128)S(1)} %get-tuple-element.554), channel_id=1, replica_groups=mesh['pp'=2,'fs'=4,'tp'=4] {'fs','tp'}, use_global_device_ids=true, to_apply=%region_2.2 | all-reduce | flops 128 | bytes 1024 | tf_op jit(solution)/shard_map/while/body/eval_jaxpr/psum | solution.py:52
  247.1 33.5 %all_gather.16 = bf16[128,2048]{1,0:T(8,128)(2,1)S(1)} all-gather(bf16[128,128]{1,0:T(8,128)(2,1)S(1)} %fusion.106), channel_id=1, replica_groups=mesh['pp'=2,'fs'=4,'tp'=4] {'fs','tp'}, dimensions={1}, use_global_device_ids=true | all-gather | bytes 557056 | tf_op jit(solution)/shard_map/while/body/eval_jaxpr/all_gather | solution.py:55
  280.6 1.6 conditional.6
  282.7 32.0 %all-reduce.2 = (f32[128]{0:T(128)S(1)}, f32[128]{0:T(128)S(1)}) all-reduce(f32[128]{0:T(128)S(1)} %get-tuple-element.558, f32[128]{0:T(128)S(1)} %get-tuple-element.559), channel_id=1, replica_groups=mesh['pp'=2,'fs'=4,'tp'=4] {'fs','tp'}, use_global_device_ids=true, to_apply=%region_10.10 | all-reduce | flops 256 | bytes 2048 | tf_op jit(solution)/shard_map/while/body/eval_jaxpr/psum | solution.py:72
  314.8 4.2 collective-permute-start
  319.1 1.6 collective-permute-done
  320.8 29.8 %psum.46 = f32[128]{0:T(128)S(1)} all-reduce(f32[128]{0:T(128)S(1)} %get-tuple-element.554), channel_id=1, replica_groups=mesh['pp'=2,'fs'=4,'tp'=4] {'fs','tp'}, use_global_device_ids=true, to_apply=%region_2.2 | all-reduce | flops 128 | bytes 1024 | tf_op jit(solution)/shard_map/while/body/eval_jaxpr/psum | solution.py:52
  350.7 36.8 %all_gather.16 = bf16[128,2048]{1,0:T(8,128)(2,1)S(1)} all-gather(bf16[128,128]{1,0:T(8,128)(2,1)S(1)} %fusion.106), channel_id=1, replica_groups=mesh['pp'=2,'fs'=4,'tp'=4] {'fs','tp'}, dimensions={1}, use_global_device_ids=true | all-gather | bytes 557056 | tf_op jit(solution)/shard_map/while/body/eval_jaxpr/all_gather | solution.py:55
  387.5 1.6 conditional.6
  389.6 29.7 %all-reduce.2 = (f32[128]{0:T(128)S(1)}, f32[128]{0:T(128)S(1)}) all-reduce(f32[128]{0:T(128)S(1)} %get-tuple-element.558, f32[128]{0:T(128)S(1)} %get-tuple-element.559), channel_id=1, replica_groups=mesh['pp'=2,'fs'=4,'tp'=4] {'fs','tp'}, use_global_device_ids=true, to_apply=%region_10.10 | all-reduce | flops 256 | bytes 2048 | tf_op jit(solution)/shard_map/while/body/eval_jaxpr/psum | solution.py:72
  419.5 4.2 collective-permute-start
  423.7 1.6 collective-permute-done
  425.4 32.0 %psum.46 = f32[128]{0:T(128)S(1)} all-reduce(f32[128]{0:T(128)S(1)} %get-tuple-element.554), channel_id=1, replica_groups=mesh['pp'=2,'fs'=4,'tp'=4] {'fs','tp'}, use_global_device_ids=true, to_apply=%region_2.2 | all-reduce | flops 128 | bytes 1024 | tf_op jit(solution)/shard_map/while/body/eval_jaxpr/psum | solution.py:52
  457.5 33.3 %all_gather.16 = bf16[128,2048]{1,0:T(8,128)(2,1)S(1)} all-gather(bf16[128,128]{1,0:T(8,128)(2,1)S(1)} %fusion.106), channel_id=1, replica_groups=mesh['pp'=2,'fs'=4,'tp'=4] {'fs','tp'}, dimensions={1}, use_global_device_ids=true | all-gather | bytes 557056 | tf_op jit(solution)/shard_map/while/body/eval_jaxpr/all_gather | solution.py:55
  491.1 32.0 %all-reduce.2 = (f32[128]{0:T(128)S(1)}, f32[128]{0:T(128)S(1)}) all-reduce(f32[128]{0:T(128)S(1)} %get-tuple-element.558, f32[128]{0:T(128)S(1)} %get-tuple-element.559), channel_id=1, replica_groups=mesh['pp'=2,'fs'=4,'tp'=4] {'fs','tp'}, use_global_device_ids=true, to_apply=%region_10.10 | all-reduce | flops 256 | bytes 2048 | tf_op jit(solution)/shard_map/while/body/eval_jaxpr/psum | solution.py:72
  523.2 6.1 %collective-permute-start = (bf16[128,128]{1,0:T(8,128)(2,1)S(1)}, bf16[128,128]{1,0:T(8,128)(2,1)S(1)}, u32[]{:S(2)}, u32[]{:S(2)}) collective-permute-start(bf16[128,128]{1,0:T(8,128)(2,1)S(1)} %get-tuple-element.564), channel_id=1, source_target_pairs={{0,16},{1,17},{2,18},{3,19},{4,20},{5,21},{6,22},{7,23},{8,24},{9,... | collective-permute-start | bytes 98312 | tf_op jit(solution)/shard_map/while/body/eval_jaxpr/ppermute | solution.py:14
  529.3 1.7 collective-permute-done
  531.0 8.0 %all_to_all.5 = bf16[2,256,128]{2,1,0:T(8,128)(2,1)S(1)} all-to-all(bf16[2,256,128]{2,1,0:T(8,128)(2,1)S(1)} %bitcast.83), channel_id=1, replica_groups=mesh['pp'=2,'fs'=4,'tp'=4] {'pp'}, dimensions={0} | all-to-all | bytes 262144 | tf_op jit(solution)/shard_map/all_to_all | solution.py:111
  (97 shorter events, 12.5 us)
Async XLA Ops:
  0.0 6.3 %copy-start.3 = (bf16[1,31,128]{2,1,0:T(8,128)(2,1)S(1)}, bf16[1,31,128]{2,1,0:T(8,128)(2,1)}, u32[]{:S(2)}) copy-start(bf16[1,31,128]{2,1,0:T(8,128)(2,1)} %param.17) | copy-start | bytes 23812
  6.3 0.7 copy-start.1
  6.3 0.7 copy-start.2
  6.3 0.7 copy-start.4
  7.0 66.5 %copy-start = (bf16[2048,128]{1,0:T(8,128)(2,1)S(1)}, bf16[2048,128]{1,0:T(8,128)(2,1)}, u32[]{:S(2)}) copy-start(bf16[2048,128]{1,0:T(8,128)(2,1)} %get-tuple-element.619) | copy-start | bytes 1572868 | tf_op jit(solution)/shard_map/while
  107.1 3.2 collective-permute-start
  110.4 66.8 %copy-start = (bf16[2048,128]{1,0:T(8,128)(2,1)S(1)}, bf16[2048,128]{1,0:T(8,128)(2,1)}, u32[]{:S(2)}) copy-start(bf16[2048,128]{1,0:T(8,128)(2,1)} %get-tuple-element.619) | copy-start | bytes 1572868 | tf_op jit(solution)/shard_map/while
  209.1 5.8 %collective-permute-start = (bf16[128,128]{1,0:T(8,128)(2,1)S(1)}, bf16[128,128]{1,0:T(8,128)(2,1)S(1)}, u32[]{:S(2)}, u32[]{:S(2)}) collective-permute-start(bf16[128,128]{1,0:T(8,128)(2,1)S(1)} %get-tuple-element.564), channel_id=1, source_target_pairs={{0,16},{1,17},{2,18},{3,19},{4,20},{5,21},{6,22},{7,23},{8,24},{9,... | collective-permute-start | bytes 98312 | tf_op jit(solution)/shard_map/while/body/eval_jaxpr/ppermute | solution.py:14
  214.9 65.7 %copy-start = (bf16[2048,128]{1,0:T(8,128)(2,1)S(1)}, bf16[2048,128]{1,0:T(8,128)(2,1)}, u32[]{:S(2)}) copy-start(bf16[2048,128]{1,0:T(8,128)(2,1)} %get-tuple-element.619) | copy-start | bytes 1572868 | tf_op jit(solution)/shard_map/while
  314.8 5.8 %collective-permute-start = (bf16[128,128]{1,0:T(8,128)(2,1)S(1)}, bf16[128,128]{1,0:T(8,128)(2,1)S(1)}, u32[]{:S(2)}, u32[]{:S(2)}) collective-permute-start(bf16[128,128]{1,0:T(8,128)(2,1)S(1)} %get-tuple-element.564), channel_id=1, source_target_pairs={{0,16},{1,17},{2,18},{3,19},{4,20},{5,21},{6,22},{7,23},{8,24},{9,... | collective-permute-start | bytes 98312 | tf_op jit(solution)/shard_map/while/body/eval_jaxpr/ppermute | solution.py:14
  320.6 66.9 %copy-start = (bf16[2048,128]{1,0:T(8,128)(2,1)S(1)}, bf16[2048,128]{1,0:T(8,128)(2,1)}, u32[]{:S(2)}) copy-start(bf16[2048,128]{1,0:T(8,128)(2,1)} %get-tuple-element.619) | copy-start | bytes 1572868 | tf_op jit(solution)/shard_map/while
  419.5 5.8 %collective-permute-start = (bf16[128,128]{1,0:T(8,128)(2,1)S(1)}, bf16[128,128]{1,0:T(8,128)(2,1)S(1)}, u32[]{:S(2)}, u32[]{:S(2)}) collective-permute-start(bf16[128,128]{1,0:T(8,128)(2,1)S(1)} %get-tuple-element.564), channel_id=1, source_target_pairs={{0,16},{1,17},{2,18},{3,19},{4,20},{5,21},{6,22},{7,23},{8,24},{9,... | collective-permute-start | bytes 98312 | tf_op jit(solution)/shard_map/while/body/eval_jaxpr/ppermute | solution.py:14
  425.3 65.6 %copy-start = (bf16[2048,128]{1,0:T(8,128)(2,1)S(1)}, bf16[2048,128]{1,0:T(8,128)(2,1)}, u32[]{:S(2)}) copy-start(bf16[2048,128]{1,0:T(8,128)(2,1)} %get-tuple-element.619) | copy-start | bytes 1572868 | tf_op jit(solution)/shard_map/while
  523.2 7.8 %collective-permute-start = (bf16[128,128]{1,0:T(8,128)(2,1)S(1)}, bf16[128,128]{1,0:T(8,128)(2,1)S(1)}, u32[]{:S(2)}, u32[]{:S(2)}) collective-permute-start(bf16[128,128]{1,0:T(8,128)(2,1)S(1)} %get-tuple-element.564), channel_id=1, source_target_pairs={{0,16},{1,17},{2,18},{3,19},{4,20},{5,21},{6,22},{7,23},{8,24},{9,... | collective-permute-start | bytes 98312 | tf_op jit(solution)/shard_map/while/body/eval_jaxpr/ppermute | solution.py:14
where the time goes:
time: 540 us
  blocking collectives  499 us (92%)
  starting transfers between devices  20.4 us (4%)
  waiting for transfers between devices  8.02 us (1%)
  matrix products  6.45 us (1%)
    all_gather x5, blocking collectives, process_block(): shard_piece = lax.all_gather(normed, ('fs', 'tp'), axis=1, tiled=True)  173 us
    psum x5, blocking collectives, process_block(): squares = lax.psum(jnp.sum(stream_f * stream_f, axis=1), ('fs', 'tp'))  157 us
    psum x5, blocking collectives, process_block(): lax.psum((jnp.sum(convolved, axis=1), jnp.sum(convolved * convolved, axis...  155 us
    ppermute x5, starting transfers between devices, from_behind(): return lax.ppermute(block, axis, route)  20.4 us
  transfers between devices with their start and end apart: 5, of which 5 were waited for; matrix products, arithmetic and copies ran while one was open for 0% of the time, Pallas kernels for 0%

commit v1 on v0

--- a/solution.py
+++ b/solution.py
@@ -70,7 +70,8 @@
             active, jnp.concatenate([history, gated_rows], axis=0)[block_rows:], history
         )
         moments = lax.psum(
-            (jnp.sum(convolved, axis=1), jnp.sum(convolved * convolved, axis=1)), ("fs", "tp")
+            lax.psum((jnp.sum(convolved, axis=1), jnp.sum(convolved * convolved, axis=1)), "tp"),
+            "fs",
         )
         row_mean = moments[0][:, None] / model_width
         row_var = moments[1][:, None] / model_width - row_mean * row_mean

time: 540 us -> 462 us (0.86)
  blocking collectives: 499 us -> 421 us
    psum x5, blocking collectives: 155 us -> 48.2 us  [process_block(): lax.psum((jnp.sum(convolved, axis=1), jnp.sum(convolved * convolved, axis...]
    psum x0 -> x5, blocking collectives: none -> 28.2 us  [process_block(): lax.psum(lax.psum((jnp.sum(convolved, axis=1), jnp.sum(convolved * convol...]
where the time goes in v1:
time: 462 us; the launch traced here: 461 us
  blocking collectives  421 us (91%)
  starting transfers between devices  20.6 us (4%)
  waiting for transfers between devices  7.87 us (2%)
  matrix products  6.46 us (1%)
    all_gather x5, blocking collectives, process_block(): shard_piece = lax.all_gather(normed, ('fs', 'tp'), axis=1, tiled=True)  174 us
    psum x5, blocking collectives, process_block(): squares = lax.psum(jnp.sum(stream_f * stream_f, axis=1), ('fs', 'tp'))  156 us
    psum x5, blocking collectives, process_block(): lax.psum((jnp.sum(convolved, axis=1), jnp.sum(convolved * convolved, axis...  48.2 us
    psum x5, blocking collectives, process_block(): lax.psum(lax.psum((jnp.sum(convolved, axis=1), jnp.sum(convolved * convol...  28.2 us
    ppermute x5, starting transfers between devices, from_behind(): return lax.ppermute(block, axis, route)  20.6 us
  transfers between devices with their start and end apart: 5, of which 5 were waited for; matrix products, arithmetic and copies ran while one was open for 0% of the time, Pallas kernels for 0%

profile of v1, /device:TPU:0, one launch (start us, length us, event | category | flops | bytes accessed | tf_op | source)
XLA Modules:
  0.0 461.1 jit_solution(4075061676413383717)
XLA Ops:
  0.0 6.3 %all_gather.13 = bf16[512,128]{1,0:T(8,128)(2,1)S(1)} all-gather(bf16[256,128]{1,0:T(8,128)(2,1)} %param.13), channel_id=1, replica_groups=mesh['pp'=2,'fs'=4,'tp'=4] {'pp'}, dimensions={0}, use_global_device_ids=true | all-gather | bytes 196608 | tf_op jit(solution)/shard_map/all_gather | solution.py:23
  7.0 445.6 %while.20 = (s32[]{:T(128)}, bf16[128,128]{1,0:T(8,128)(2,1)S(1)}, f32[30,128]{1,0:T(8,128)S(1)}, bf16[512,128]{1,0:T(8,128)(2,1)S(1)}, s32[]{:T(128)}, /*index=...) while((s32[]{:T(128)}, bf16[128,128]{1,0:T(8,128)(2,1)S(1)}, ...), condition=%wide.region_13.14_spmd.clone, body=%wide.region_0.13_spmd.clone.sunk | while | flops 136180240 | bytes 5905606 | solution.py:109
  7.1 33.1 %psum.76 = f32[128]{0:T(128)S(1)} all-reduce(f32[128]{0:T(128)S(1)} %get-tuple-element.558), channel_id=1, replica_groups=mesh['pp'=2,'fs'=4,'tp'=4] {'fs','tp'}, use_global_device_ids=true, to_apply=%region_2.2 | all-reduce | flops 128 | bytes 1024 | tf_op jit(solution)/shard_map/while/body/eval_jaxpr/psum | solution.py:52
  40.3 33.2 %all_gather.16 = bf16[128,2048]{1,0:T(8,128)(2,1)S(1)} all-gather(bf16[128,128]{1,0:T(8,128)(2,1)S(1)} %fusion.106), channel_id=1, replica_groups=mesh['pp'=2,'fs'=4,'tp'=4] {'fs','tp'}, dimensions={1}, use_global_device_ids=true | all-gather | bytes 557056 | tf_op jit(solution)/shard_map/while/body/eval_jaxpr/all_gather | solution.py:55
  73.5 1.6 conditional.6
  75.6 10.1 %all-reduce.4 = (f32[128]{0:T(128)S(1)}, f32[128]{0:T(128)S(1)}) all-reduce(f32[128]{0:T(128)S(1)} %get-tuple-element.562, f32[128]{0:T(128)S(1)} %get-tuple-element.563), channel_id=1, replica_groups=mesh['pp'=2,'fs'=4,'tp'=4] {'tp'}, use_global_device_ids=true, to_apply=%region_11.11 | all-reduce | flops 256 | bytes 2048 | tf_op jit(solution)/shard_map/while/body/eval_jaxpr/psum | solution.py:73
  85.7 5.6 %all-reduce.5 = (f32[128]{0:T(128)S(1)}, f32[128]{0:T(128)S(1)}) all-reduce(f32[128]{0:T(128)S(1)} %get-tuple-element.564, f32[128]{0:T(128)S(1)} %get-tuple-element.565), channel_id=1, replica_groups=mesh['pp'=2,'fs'=4,'tp'=4] {'fs'}, use_global_device_ids=true, to_apply=%region_12.12 | all-reduce | flops 256 | bytes 2048 | tf_op jit(solution)/shard_map/while/body/eval_jaxpr/psum | solution.py:72
  91.5 1.7 collective-permute-start
  94.9 29.9 %psum.76 = f32[128]{0:T(128)S(1)} all-reduce(f32[128]{0:T(128)S(1)} %get-tuple-element.558), channel_id=1, replica_groups=mesh['pp'=2,'fs'=4,'tp'=4] {'fs','tp'}, use_global_device_ids=true, to_apply=%region_2.2 | all-reduce | flops 128 | bytes 1024 | tf_op jit(solution)/shard_map/while/body/eval_jaxpr/psum | solution.py:52
  124.8 36.9 %all_gather.16 = bf16[128,2048]{1,0:T(8,128)(2,1)S(1)} all-gather(bf16[128,128]{1,0:T(8,128)(2,1)S(1)} %fusion.106), channel_id=1, replica_groups=mesh['pp'=2,'fs'=4,'tp'=4] {'fs','tp'}, dimensions={1}, use_global_device_ids=true | all-gather | bytes 557056 | tf_op jit(solution)/shard_map/while/body/eval_jaxpr/all_gather | solution.py:55
  161.7 1.6 conditional.6
  163.8 8.4 %all-reduce.4 = (f32[128]{0:T(128)S(1)}, f32[128]{0:T(128)S(1)}) all-reduce(f32[128]{0:T(128)S(1)} %get-tuple-element.562, f32[128]{0:T(128)S(1)} %get-tuple-element.563), channel_id=1, replica_groups=mesh['pp'=2,'fs'=4,'tp'=4] {'tp'}, use_global_device_ids=true, to_apply=%region_11.11 | all-reduce | flops 256 | bytes 2048 | tf_op jit(solution)/shard_map/while/body/eval_jaxpr/psum | solution.py:73
  172.2 5.6 %all-reduce.5 = (f32[128]{0:T(128)S(1)}, f32[128]{0:T(128)S(1)}) all-reduce(f32[128]{0:T(128)S(1)} %get-tuple-element.564, f32[128]{0:T(128)S(1)} %get-tuple-element.565), channel_id=1, replica_groups=mesh['pp'=2,'fs'=4,'tp'=4] {'fs'}, use_global_device_ids=true, to_apply=%region_12.12 | all-reduce | flops 256 | bytes 2048 | tf_op jit(solution)/shard_map/while/body/eval_jaxpr/psum | solution.py:72
  178.0 4.2 collective-permute-start
  183.9 31.8 %psum.76 = f32[128]{0:T(128)S(1)} all-reduce(f32[128]{0:T(128)S(1)} %get-tuple-element.558), channel_id=1, replica_groups=mesh['pp'=2,'fs'=4,'tp'=4] {'fs','tp'}, use_global_device_ids=true, to_apply=%region_2.2 | all-reduce | flops 128 | bytes 1024 | tf_op jit(solution)/shard_map/while/body/eval_jaxpr/psum | solution.py:52
  215.8 33.5 %all_gather.16 = bf16[128,2048]{1,0:T(8,128)(2,1)S(1)} all-gather(bf16[128,128]{1,0:T(8,128)(2,1)S(1)} %fusion.106), channel_id=1, replica_groups=mesh['pp'=2,'fs'=4,'tp'=4] {'fs','tp'}, dimensions={1}, use_global_device_ids=true | all-gather | bytes 557056 | tf_op jit(solution)/shard_map/while/body/eval_jaxpr/all_gather | solution.py:55
  249.3 1.6 conditional.6
  251.4 10.7 %all-reduce.4 = (f32[128]{0:T(128)S(1)}, f32[128]{0:T(128)S(1)}) all-reduce(f32[128]{0:T(128)S(1)} %get-tuple-element.562, f32[128]{0:T(128)S(1)} %get-tuple-element.563), channel_id=1, replica_groups=mesh['pp'=2,'fs'=4,'tp'=4] {'tp'}, use_global_device_ids=true, to_apply=%region_11.11 | all-reduce | flops 256 | bytes 2048 | tf_op jit(solution)/shard_map/while/body/eval_jaxpr/psum | solution.py:73
  262.1 5.6 %all-reduce.5 = (f32[128]{0:T(128)S(1)}, f32[128]{0:T(128)S(1)}) all-reduce(f32[128]{0:T(128)S(1)} %get-tuple-element.564, f32[128]{0:T(128)S(1)} %get-tuple-element.565), channel_id=1, replica_groups=mesh['pp'=2,'fs'=4,'tp'=4] {'fs'}, use_global_device_ids=true, to_apply=%region_12.12 | all-reduce | flops 256 | bytes 2048 | tf_op jit(solution)/shard_map/while/body/eval_jaxpr/psum | solution.py:72
  267.9 4.3 collective-permute-start
  273.9 29.8 %psum.76 = f32[128]{0:T(128)S(1)} all-reduce(f32[128]{0:T(128)S(1)} %get-tuple-element.558), channel_id=1, replica_groups=mesh['pp'=2,'fs'=4,'tp'=4] {'fs','tp'}, use_global_device_ids=true, to_apply=%region_2.2 | all-reduce | flops 128 | bytes 1024 | tf_op jit(solution)/shard_map/while/body/eval_jaxpr/psum | solution.py:52
  303.8 36.6 %all_gather.16 = bf16[128,2048]{1,0:T(8,128)(2,1)S(1)} all-gather(bf16[128,128]{1,0:T(8,128)(2,1)S(1)} %fusion.106), channel_id=1, replica_groups=mesh['pp'=2,'fs'=4,'tp'=4] {'fs','tp'}, dimensions={1}, use_global_device_ids=true | all-gather | bytes 557056 | tf_op jit(solution)/shard_map/while/body/eval_jaxpr/all_gather | solution.py:55
  340.4 1.6 conditional.6
  342.5 8.4 %all-reduce.4 = (f32[128]{0:T(128)S(1)}, f32[128]{0:T(128)S(1)}) all-reduce(f32[128]{0:T(128)S(1)} %get-tuple-element.562, f32[128]{0:T(128)S(1)} %get-tuple-element.563), channel_id=1, replica_groups=mesh['pp'=2,'fs'=4,'tp'=4] {'tp'}, use_global_device_ids=true, to_apply=%region_11.11 | all-reduce | flops 256 | bytes 2048 | tf_op jit(solution)/shard_map/while/body/eval_jaxpr/psum | solution.py:73
  350.9 5.6 %all-reduce.5 = (f32[128]{0:T(128)S(1)}, f32[128]{0:T(128)S(1)}) all-reduce(f32[128]{0:T(128)S(1)} %get-tuple-element.564, f32[128]{0:T(128)S(1)} %get-tuple-element.565), channel_id=1, replica_groups=mesh['pp'=2,'fs'=4,'tp'=4] {'fs'}, use_global_device_ids=true, to_apply=%region_12.12 | all-reduce | flops 256 | bytes 2048 | tf_op jit(solution)/shard_map/while/body/eval_jaxpr/psum | solution.py:72
  356.7 4.2 collective-permute-start
  362.6 31.8 %psum.76 = f32[128]{0:T(128)S(1)} all-reduce(f32[128]{0:T(128)S(1)} %get-tuple-element.558), channel_id=1, replica_groups=mesh['pp'=2,'fs'=4,'tp'=4] {'fs','tp'}, use_global_device_ids=true, to_apply=%region_2.2 | all-reduce | flops 128 | bytes 1024 | tf_op jit(solution)/shard_map/while/body/eval_jaxpr/psum | solution.py:52
  394.5 33.6 %all_gather.16 = bf16[128,2048]{1,0:T(8,128)(2,1)S(1)} all-gather(bf16[128,128]{1,0:T(8,128)(2,1)S(1)} %fusion.106), channel_id=1, replica_groups=mesh['pp'=2,'fs'=4,'tp'=4] {'fs','tp'}, dimensions={1}, use_global_device_ids=true | all-gather | bytes 557056 | tf_op jit(solution)/shard_map/while/body/eval_jaxpr/all_gather | solution.py:55
  428.4 10.7 %all-reduce.4 = (f32[128]{0:T(128)S(1)}, f32[128]{0:T(128)S(1)}) all-reduce(f32[128]{0:T(128)S(1)} %get-tuple-element.562, f32[128]{0:T(128)S(1)} %get-tuple-element.563), channel_id=1, replica_groups=mesh['pp'=2,'fs'=4,'tp'=4] {'tp'}, use_global_device_ids=true, to_apply=%region_11.11 | all-reduce | flops 256 | bytes 2048 | tf_op jit(solution)/shard_map/while/body/eval_jaxpr/psum | solution.py:73
  439.1 5.6 %all-reduce.5 = (f32[128]{0:T(128)S(1)}, f32[128]{0:T(128)S(1)}) all-reduce(f32[128]{0:T(128)S(1)} %get-tuple-element.564, f32[128]{0:T(128)S(1)} %get-tuple-element.565), channel_id=1, replica_groups=mesh['pp'=2,'fs'=4,'tp'=4] {'fs'}, use_global_device_ids=true, to_apply=%region_12.12 | all-reduce | flops 256 | bytes 2048 | tf_op jit(solution)/shard_map/while/body/eval_jaxpr/psum | solution.py:72
  444.9 6.1 %collective-permute-start = (bf16[128,128]{1,0:T(8,128)(2,1)S(1)}, bf16[128,128]{1,0:T(8,128)(2,1)S(1)}, u32[]{:S(2)}, u32[]{:S(2)}) collective-permute-start(bf16[128,128]{1,0:T(8,128)(2,1)S(1)} %get-tuple-element.570), channel_id=1, source_target_pairs={{0,16},{1,17},{2,18},{3,19},{4,20},{5,21},{6,22},{7,23},{8,24},{9,... | collective-permute-start | bytes 98312 | tf_op jit(solution)/shard_map/while/body/eval_jaxpr/ppermute | solution.py:14
  452.6 7.8 %all_to_all.5 = bf16[2,256,128]{2,1,0:T(8,128)(2,1)S(1)} all-to-all(bf16[2,256,128]{2,1,0:T(8,128)(2,1)S(1)} %bitcast.83), channel_id=1, replica_groups=mesh['pp'=2,'fs'=4,'tp'=4] {'pp'}, dimensions={0} | all-to-all | bytes 262144 | tf_op jit(solution)/shard_map/all_to_all | solution.py:112
  (102 shorter events, 20.3 us)
Async XLA Ops:
  0.0 6.3 %copy-start.3 = (bf16[1,31,128]{2,1,0:T(8,128)(2,1)S(1)}, bf16[1,31,128]{2,1,0:T(8,128)(2,1)}, u32[]{:S(2)}) copy-start(bf16[1,31,128]{2,1,0:T(8,128)(2,1)} %param.17) | copy-start | bytes 23812
  6.3 0.7 copy-start.1
  6.3 0.7 copy-start.2
  6.3 0.7 copy-start.4
  7.0 66.5 %copy-start = (bf16[2048,128]{1,0:T(8,128)(2,1)S(1)}, bf16[2048,128]{1,0:T(8,128)(2,1)}, u32[]{:S(2)}) copy-start(bf16[2048,128]{1,0:T(8,128)(2,1)} %get-tuple-element.625) | copy-start | bytes 1572868 | tf_op jit(solution)/shard_map/while
  91.5 3.3 collective-permute-start
  94.7 67.0 %copy-start = (bf16[2048,128]{1,0:T(8,128)(2,1)S(1)}, bf16[2048,128]{1,0:T(8,128)(2,1)}, u32[]{:S(2)}) copy-start(bf16[2048,128]{1,0:T(8,128)(2,1)} %get-tuple-element.625) | copy-start | bytes 1572868 | tf_op jit(solution)/shard_map/while
  178.0 5.8 %collective-permute-start = (bf16[128,128]{1,0:T(8,128)(2,1)S(1)}, bf16[128,128]{1,0:T(8,128)(2,1)S(1)}, u32[]{:S(2)}, u32[]{:S(2)}) collective-permute-start(bf16[128,128]{1,0:T(8,128)(2,1)S(1)} %get-tuple-element.570), channel_id=1, source_target_pairs={{0,16},{1,17},{2,18},{3,19},{4,20},{5,21},{6,22},{7,23},{8,24},{9,... | collective-permute-start | bytes 98312 | tf_op jit(solution)/shard_map/while/body/eval_jaxpr/ppermute | solution.py:14
  183.8 65.5 %copy-start = (bf16[2048,128]{1,0:T(8,128)(2,1)S(1)}, bf16[2048,128]{1,0:T(8,128)(2,1)}, u32[]{:S(2)}) copy-start(bf16[2048,128]{1,0:T(8,128)(2,1)} %get-tuple-element.625) | copy-start | bytes 1572868 | tf_op jit(solution)/shard_map/while
  267.9 5.9 %collective-permute-start = (bf16[128,128]{1,0:T(8,128)(2,1)S(1)}, bf16[128,128]{1,0:T(8,128)(2,1)S(1)}, u32[]{:S(2)}, u32[]{:S(2)}) collective-permute-start(bf16[128,128]{1,0:T(8,128)(2,1)S(1)} %get-tuple-element.570), channel_id=1, source_target_pairs={{0,16},{1,17},{2,18},{3,19},{4,20},{5,21},{6,22},{7,23},{8,24},{9,... | collective-permute-start | bytes 98312 | tf_op jit(solution)/shard_map/while/body/eval_jaxpr/ppermute | solution.py:14
  273.8 66.6 %copy-start = (bf16[2048,128]{1,0:T(8,128)(2,1)S(1)}, bf16[2048,128]{1,0:T(8,128)(2,1)}, u32[]{:S(2)}) copy-start(bf16[2048,128]{1,0:T(8,128)(2,1)} %get-tuple-element.625) | copy-start | bytes 1572868 | tf_op jit(solution)/shard_map/while
  356.7 5.8 %collective-permute-start = (bf16[128,128]{1,0:T(8,128)(2,1)S(1)}, bf16[128,128]{1,0:T(8,128)(2,1)S(1)}, u32[]{:S(2)}, u32[]{:S(2)}) collective-permute-start(bf16[128,128]{1,0:T(8,128)(2,1)S(1)} %get-tuple-element.570), channel_id=1, source_target_pairs={{0,16},{1,17},{2,18},{3,19},{4,20},{5,21},{6,22},{7,23},{8,24},{9,... | collective-permute-start | bytes 98312 | tf_op jit(solution)/shard_map/while/body/eval_jaxpr/ppermute | solution.py:14
  362.5 65.7 %copy-start = (bf16[2048,128]{1,0:T(8,128)(2,1)S(1)}, bf16[2048,128]{1,0:T(8,128)(2,1)}, u32[]{:S(2)}) copy-start(bf16[2048,128]{1,0:T(8,128)(2,1)} %get-tuple-element.625) | copy-start | bytes 1572868 | tf_op jit(solution)/shard_map/while
  444.9 7.7 %collective-permute-start = (bf16[128,128]{1,0:T(8,128)(2,1)S(1)}, bf16[128,128]{1,0:T(8,128)(2,1)S(1)}, u32[]{:S(2)}, u32[]{:S(2)}) collective-permute-start(bf16[128,128]{1,0:T(8,128)(2,1)S(1)} %get-tuple-element.570), channel_id=1, source_target_pairs={{0,16},{1,17},{2,18},{3,19},{4,20},{5,21},{6,22},{7,23},{8,24},{9,... | collective-permute-start | bytes 98312 | tf_op jit(solution)/shard_map/while/body/eval_jaxpr/ppermute | solution.py:14
